TPU v7x, 32 devices: a whole 2x2x4 slice. The times are simulated.
32 devices in a mesh: sp: 8 (over z, y), tp: 4 (over x, core).
Axes of the slice: x: 2, y: 2, z: 4, core: 2. Of those that a mesh axis runs over, the one named last changes fastest.
Arguments:
- tokens: bfloat16 [16384, 2048], P('sp'), may hold values from -6 to 6
- w_query: bfloat16 [2048, 1024], P(None, 'tp'), may hold values from -0.125 to 0.125
- w_key: bfloat16 [2048, 1024], P(None, 'tp'), may hold values from -0.125 to 0.125
- w_value: bfloat16 [2048, 1024], P(None, 'tp'), may hold values from -0.125 to 0.125
- w_gate: bfloat16 [2048, 1024], P(None, 'tp'), may hold values from -0.125 to 0.125
- w_pool: bfloat16 [2048, 1024], P(None, 'tp'), may hold values from -0.125 to 0.125
- norm_gain: float32 [1024], P('tp'), may hold values from 0.1 to 1.9
- log_decay: float32 [8, 16384], P('tp', 'sp'), may hold values from -0.8 to 0
- w_out: bfloat16 [2048, 2048], replicated, may hold values from -0.125 to 0.125
Outputs:
- mixed_out: bfloat16 [16384, 2048], P(('sp', 'tp'))
All inputs are finite; a program needn't handle non-finite values.
Results may differ from a plain program's by a relative error of at most 0.014.
Values may be sent and summed in bfloat16 or wider, within the bound.
A program may use at most 64 MiB of HBM per device.

v0:
```python
import functools

import jax
import jax.numpy as jnp
import numpy as np
from jax import lax
from jax.experimental import pallas as pl
from jax.experimental.pallas import tpu as pltpu
from jax.sharding import PartitionSpec as P

HEAD_DIM = 128
POOL_GROUP = 256
BLOCK = 128
CHUNK = 256
HALO = 16
F32 = jnp.float32
BF16 = jnp.bfloat16
MESH = pl.DeviceIdType.MESH


def mm(a, b):
    return jnp.dot(a, b, preferred_element_type=F32)


def rotary_tables(n_blocks):
    half = HEAD_DIM // 2
    inverse = 10000.0 ** (-np.arange(half, dtype=np.float64) / half)
    starts = (np.arange(n_blocks) * BLOCK)[:, None] * inverse[None, :]
    offsets = np.arange(BLOCK)[:, None] * inverse[None, :]

    def pair(angles):
        cosine, sine = np.cos(angles), np.sin(angles)
        return (
            np.concatenate([cosine, cosine], 1).astype(np.float32),
            np.concatenate([-sine, sine], 1).astype(np.float32),
        )

    return *pair(starts), *pair(offsets)


def kernel(
    sp_n, tp_n,
    tokens, wq, wk, wv, wg, wp, gain, log_decay, wout, cos_b, sin_b, cos_r, sin_r,
    out,
    tok_v, wq_v, wk_v, wv_v, wg_v, wp_v, wout_v,
    ld_s, cum_s, bend_s, reach_s, col_s,
    k_s, v_s, q_s, g_s, pool_s, inner_s, before_s, state_s,
    st_send, st_recv, tot_send, tot_recv, rim_recv, inc_s,
    pooled_s, gated_s, gath, acc_s,
    tok_sem, w_sem, st_ssem, st_rsem, tot_ssem, tot_rsem, rim_sem, mix_ssem, mix_rsem,
):
    sp = lax.axis_index("sp")
    tp = lax.axis_index("tp")
    rows = tok_v.shape[0]
    heads = k_s.shape[1] // HEAD_DIM
    pool_cols = pool_s.shape[1]
    ret_width = tp_n * heads * HEAD_DIM
    n_blocks = rows // BLOCK
    n_chunks = rows // CHUNK
    per_chunk = CHUNK // BLOCK
    rows_out = rows // tp_n
    pieces = rows_out // CHUNK
    chips = tp_n // 2
    scale = HEAD_DIM ** (-0.5)

    barrier = pltpu.get_barrier_semaphore()

    def load(src, dst, sem):
        return pltpu.make_async_copy(src, dst, sem)

    def tok_copy(c):
        r = pl.ds(pl.multiple_of(c * CHUNK, CHUNK), CHUNK)
        return load(tokens.at[r], tok_v.at[r], tok_sem.at[c])

    load_k = load(wk, wk_v, w_sem.at[0])
    load_v = load(wv, wv_v, w_sem.at[1])
    load_p = load(wp, wp_v, w_sem.at[2])
    load_q = load(wq, wq_v, w_sem.at[3])
    load_g = load(wg, wg_v, w_sem.at[4])
    load_o = load(wout, wout_v, w_sem.at[5])
    load_k.start()
    tok_copy(0).start()
    load_v.start()

    def start_tok(c, carry):
        tok_copy(c).start()
        return carry

    lax.fori_loop(1, n_chunks, start_tok, 0)
    load_p.start()

    def greet_sp(d, carry):
        pl.semaphore_signal(barrier, inc=1, device_id=((sp + d) % sp_n, tp), device_id_type=MESH)
        return carry

    def greet_tp(d, carry):
        pl.semaphore_signal(barrier, inc=1, device_id=(sp, (tp + d) % tp_n), device_id_type=MESH)
        return carry

    lax.fori_loop(1, sp_n, greet_sp, 0)
    lax.fori_loop(1, tp_n, greet_tp, 0)

    for n in range(n_blocks):
        ld_s[n * heads : (n + 1) * heads, :] = log_decay[:, n * BLOCK : (n + 1) * BLOCK]
    t_iota = lax.broadcasted_iota(jnp.int32, (BLOCK, BLOCK), 0)
    s_iota = lax.broadcasted_iota(jnp.int32, (BLOCK, BLOCK), 1)
    causal = t_iota >= s_iota
    upper = jnp.where(t_iota <= s_iota, 1.0, 0.0).astype(F32)
    ld = ld_s[...]
    cum_s[...] = jnp.dot(ld, upper, preferred_element_type=F32, precision=lax.Precision.HIGHEST)
    bend_s[...] = jnp.dot(
        ld, jnp.ones((BLOCK, BLOCK), F32), preferred_element_type=F32,
        precision=lax.Precision.HIGHEST,
    )
    run = jnp.zeros((heads, HEAD_DIM), F32)
    for n in range(n_blocks):
        reach_s[n * heads : (n + 1) * heads, :] = jnp.exp(run)
        run = run + bend_s[n * heads : (n + 1) * heads, :]
    tot_send[...] = jnp.zeros_like(tot_send)
    tot_send[0:heads, :] = jnp.exp(run)
    state_s[...] = jnp.zeros_like(state_s)
    load_k.wait()
    load_v.wait()

    def angles(n):
        at = pl.ds(sp * n_blocks + n, 1)
        cb, sb = cos_b[at, :], sin_b[at, :]
        cr, sr = cos_r[...], sin_r[...]
        return cb * cr - sb * sr, sb * cr + cb * sr

    def turned(x, cosine, sine):
        return x * cosine + pltpu.roll(x, HEAD_DIM // 2, 1) * sine

    def chunk_rows(c):
        return pl.ds(pl.multiple_of(c * CHUNK, CHUNK), CHUNK)

    def block_rows(n):
        return pl.ds(pl.multiple_of(n * BLOCK, BLOCK), BLOCK)

    def kv_chunk(c, carry):
        tok_copy(c).wait()
        x = tok_v[chunk_rows(c), :]
        key = mm(x, wk_v[...]).astype(BF16).astype(F32)
        value = mm(x, wv_v[...]).astype(BF16)
        v_s[chunk_rows(c), :] = value
        for b in range(per_chunk):
            n = c * per_chunk + b
            cosine, sine = angles(n)
            for h in range(heads):
                cols = slice(h * HEAD_DIM, (h + 1) * HEAD_DIM)
                part = slice(b * BLOCK, (b + 1) * BLOCK)
                k_rot = (turned(key[part, cols], cosine, sine) * scale).astype(BF16)
                k_s[block_rows(n), cols] = k_rot
                at = n * heads + h
                col = jnp.broadcast_to(cum_s[pl.ds(at, 1), :], (BLOCK, BLOCK)).T
                col_s[at] = col
                end = bend_s[pl.ds(at, 1), :]
                decayed = (k_rot.astype(F32) * jnp.exp(end - col)).astype(BF16)
                update = lax.dot_general(
                    decayed, value[part, cols], (((0,), (0,)), ((), ())),
                    preferred_element_type=F32,
                )
                state = state_s[h]
                before_s[at] = state
                state_s[h] = state * jnp.exp(end) + update
        return carry

    lax.fori_loop(0, n_chunks, kv_chunk, 0)
    load_q.start()
    load_g.start()
    load_o.start()
    for h in range(heads):
        st_send[h] = state_s[h].astype(BF16)

    pl.semaphore_wait(barrier, sp_n - 1 + tp_n - 1)

    def state_copies(d):
        target = ((sp + d) % sp_n, tp)
        return (
            pltpu.make_async_remote_copy(
                src_ref=tot_send, dst_ref=tot_recv.at[sp], send_sem=tot_ssem.at[d],
                recv_sem=tot_rsem.at[sp], device_id=target, device_id_type=MESH,
            ),
            pltpu.make_async_remote_copy(
                src_ref=st_send, dst_ref=st_recv.at[sp], send_sem=st_ssem.at[d],
                recv_sem=st_rsem.at[sp], device_id=target, device_id_type=MESH,
            ),
        )

    def send_state(d, carry):
        for copy in state_copies(d):
            copy.start()
        return carry

    def sent_state(d, carry):
        for copy in state_copies(d):
            copy.wait_send()
        return carry

    lax.fori_loop(1, sp_n - sp, send_state, 0)

    load_p.wait()

    def pool_chunk(c):
        at = pl.ds(pl.multiple_of(HALO + c * CHUNK, HALO), CHUNK)
        pool_s[at, :] = mm(tok_v[chunk_rows(c), :], wp_v[...]).astype(BF16)

    pool_chunk(n_chunks - 1)
    rim = pltpu.make_async_remote_copy(
        src_ref=pool_s.at[pl.ds(rows, HALO)], dst_ref=rim_recv, send_sem=rim_sem.at[0],
        recv_sem=rim_sem.at[1], device_id=((sp + 1) % sp_n, tp), device_id_type=MESH,
    )

    @pl.when(sp < sp_n - 1)
    def _():
        rim.start()

    def pool_step(c, carry):
        pool_chunk(c)
        return carry

    lax.fori_loop(0, n_chunks - 1, pool_step, 0)

    @pl.when(sp == 0)
    def _():
        pool_s[0:HALO, :] = jnp.zeros((HALO, pool_cols), BF16)

    @pl.when(sp > 0)
    def _():
        rim.wait_recv()
        pool_s[0:HALO, :] = rim_recv[...]

    def target_of(t):
        chip = (tp // 2 + 1 + t // (2 * pieces)) % chips
        piece = (t % (2 * pieces)) // 2
        dest = chip * 2 + (tp + t + 1) % 2
        return dest, piece, dest * pieces + piece

    def mix_copy(kind, t):
        dest, piece, c = target_of(t)
        src = (gated_s, pooled_s)[kind]
        width = src.shape[1]
        first = pl.multiple_of(kind * ret_width + tp * width, HEAD_DIM)
        return pltpu.make_async_remote_copy(
            src_ref=src.at[chunk_rows(c)],
            dst_ref=gath.at[chunk_rows(piece), pl.ds(first, width)],
            send_sem=mix_ssem.at[kind, t],
            recv_sem=mix_rsem.at[kind, tp, piece],
            device_id=(sp, dest), device_id_type=MESH,
        )

    def hand_over(kind, t, block):
        dest, piece, c = target_of(t)
        dst = (gated_s, pooled_s)[kind]
        width = dst.shape[1]
        first = pl.multiple_of(kind * ret_width + tp * width, HEAD_DIM)

        @pl.when(dest == tp)
        def _():
            gath[chunk_rows(piece), pl.ds(first, width)] = block

        @pl.when(dest != tp)
        def _():
            dst[chunk_rows(c), :] = block
            mix_copy(kind, t).start()

    group = (tp * pool_cols) // POOL_GROUP
    window = lax.shift_left(jnp.int32(2), group.astype(jnp.int32))
    gap = (
        lax.broadcasted_iota(jnp.int32, (CHUNK, CHUNK + HALO), 0)
        + HALO
        - lax.broadcasted_iota(jnp.int32, (CHUNK, CHUNK + HALO), 1)
    )
    band = jnp.where((gap >= 0) & (gap < window), 1.0, 0.0).astype(BF16)
    row_iota = lax.broadcasted_iota(jnp.int32, (CHUNK, pool_cols), 0)

    def pool_send(t, carry):
        _, _, c = target_of(t)
        at = pl.ds(pl.multiple_of(c * CHUNK, CHUNK), CHUNK + HALO)
        sums = mm(band, pool_s[at, :])
        own = pool_s[pl.ds(pl.multiple_of(HALO + c * CHUNK, HALO), CHUNK), :].astype(F32)
        count = jnp.minimum(sp * rows + c * CHUNK + row_iota + 1, window).astype(F32)
        hand_over(1, t, (sums / count - own).astype(BF16))
        return carry

    lax.fori_loop(0, n_chunks, pool_send, 0)

    load_q.wait()
    load_g.wait()

    def q_chunk(c, carry):
        x = tok_v[chunk_rows(c), :]
        query = mm(x, wq_v[...]).astype(BF16).astype(F32)
        g_s[chunk_rows(c), :] = mm(x, wg_v[...]).astype(BF16)
        for b in range(per_chunk):
            n = c * per_chunk + b
            cosine, sine = angles(n)
            for h in range(heads):
                cols = slice(h * HEAD_DIM, (h + 1) * HEAD_DIM)
                q_rot = turned(query[b * BLOCK : (b + 1) * BLOCK, cols], cosine, sine).astype(BF16)
                q_s[block_rows(n), cols] = q_rot
                at = n * heads + h
                fade = jnp.exp(jnp.minimum(col_s[at] - cum_s[pl.ds(at, 1), :], 0.0))
                scores = lax.dot_general(
                    q_rot, k_s[block_rows(n), cols], (((1,), (1,)), ((), ())),
                    preferred_element_type=F32,
                )
                mixing = (scores * jnp.where(causal, fade, 0.0)).astype(BF16)
                inner_s[block_rows(n), cols] = mm(mixing, v_s[block_rows(n), cols])
        return carry

    lax.fori_loop(0, n_chunks, q_chunk, 0)

    inc_s[...] = jnp.zeros_like(inc_s)

    def enter(i, carry):
        tot_in = pltpu.make_async_copy(tot_recv.at[i], tot_recv.at[i], tot_rsem.at[i])
        st_in = pltpu.make_async_copy(st_recv.at[i], st_recv.at[i], st_rsem.at[i])
        tot_in.wait()
        st_in.wait()
        for h in range(heads):
            inc_s[h] = inc_s[h] * tot_recv[i, h : h + 1, :] + st_recv[i, h].astype(F32)
        return carry

    lax.fori_loop(0, sp, enter, 0)

    def ret_send(t, carry):
        _, _, c = target_of(t)
        parts = []
        for b in range(per_chunk):
            n = c * per_chunk + b
            line = []
            for h in range(heads):
                cols = slice(h * HEAD_DIM, (h + 1) * HEAD_DIM)
                at = n * heads + h
                state = (before_s[at] + reach_s[pl.ds(at, 1), :] * inc_s[h]).astype(BF16)
                cross = mm(q_s[block_rows(n), cols], state) * jnp.exp(col_s[at])
                kept = inner_s[block_rows(n), cols] + cross
                centered = kept - jnp.mean(kept, axis=-1, keepdims=True)
                power = jnp.mean(centered * centered, axis=-1, keepdims=True)
                normed = centered * lax.rsqrt(power + 1e-06)
                gate = g_s[block_rows(n), cols].astype(F32)
                line.append((jax.nn.silu(gate) * gain[:, cols] * normed).astype(BF16))
            parts.append(jnp.concatenate(line, axis=1) if heads > 1 else line[0])
        hand_over(0, t, jnp.concatenate(parts, axis=0))
        return carry

    lax.fori_loop(0, n_chunks, ret_send, 0)

    load_o.wait()

    def arrived(kind, src, piece):
        width = (gated_s, pooled_s)[kind].shape[1]
        here = gath.at[
            chunk_rows(piece), pl.ds(pl.multiple_of(kind * ret_width + src * width, HEAD_DIM), width)
        ]
        pltpu.make_async_copy(here, here, mix_rsem.at[kind, src, piece]).wait()

    def wait_piece(kind, piece):
        def one(d, carry):
            arrived(kind, (tp + d) % tp_n, piece)
            return carry

        lax.fori_loop(1, tp_n, one, 0)

    width_out = wout_v.shape[1]
    tile = min(512, width_out)

    def tile_cols(j):
        return pl.ds(pl.multiple_of(j * tile, tile), tile)

    def pool_out(piece, carry):
        wait_piece(1, piece)

        def one(j, carry):
            acc_s[chunk_rows(piece), tile_cols(j)] = mm(
                gath[chunk_rows(piece), ret_width:], wout_v[ret_width:, tile_cols(j)]
            )
            return carry

        return lax.fori_loop(0, width_out // tile, one, carry)

    lax.fori_loop(0, pieces, pool_out, 0)

    def ret_out(piece, carry):
        wait_piece(0, piece)

        def one(j, carry):
            total = acc_s[chunk_rows(piece), tile_cols(j)] + mm(
                gath[chunk_rows(piece), :ret_width], wout_v[:ret_width, tile_cols(j)]
            )
            out[chunk_rows(piece), tile_cols(j)] = total.astype(BF16)
            return carry

        return lax.fori_loop(0, width_out // tile, one, carry)

    lax.fori_loop(0, pieces, ret_out, 0)

    lax.fori_loop(1, sp_n - sp, sent_state, 0)

    @pl.when(sp < sp_n - 1)
    def _():
        rim.wait_send()

    def sent_mix(t, carry):
        dest, _, _ = target_of(t)

        @pl.when(dest != tp)
        def _():
            mix_copy(0, t).wait_send()
            mix_copy(1, t).wait_send()

        return carry

    lax.fori_loop(0, n_chunks, sent_mix, 0)


def local(
    sp_n, tp_n, tables, tokens, w_query, w_key, w_value, w_gate, w_pool, norm_gain, log_decay, w_out
):
    rows, width = tokens.shape
    ret_cols = w_query.shape[1]
    pool_cols = w_pool.shape[1]
    heads = ret_cols // HEAD_DIM
    n_blocks = rows // BLOCK
    n_chunks = rows // CHUNK
    rows_out = rows // tp_n
    assert POOL_GROUP % pool_cols == 0 and rows_out % CHUNK == 0 and tp_n % 2 == 0
    both = n_blocks * heads
    tot_rows = -(-heads // 8) * 8
    hbm = pl.BlockSpec(memory_space=pl.ANY)
    vmem = pl.BlockSpec(memory_space=pltpu.VMEM)
    V = pltpu.VMEM
    dma = pltpu.SemaphoreType.DMA
    return pl.pallas_call(
        functools.partial(kernel, sp_n, tp_n),
        name="layer",
        out_shape=jax.ShapeDtypeStruct((rows_out, w_out.shape[1]), BF16),
        in_specs=[hbm] * 6 + [vmem] * 2 + [hbm] + [vmem] * 4,
        out_specs=vmem,
        scratch_shapes=[
            V((rows, width), BF16),
            V((width, ret_cols), BF16),
            V((width, ret_cols), BF16),
            V((width, ret_cols), BF16),
            V((width, ret_cols), BF16),
            V((width, pool_cols), BF16),
            V(w_out.shape, BF16),
            V((both, BLOCK), F32),
            V((both, BLOCK), F32),
            V((both, BLOCK), F32),
            V((both, BLOCK), F32),
            V((both, BLOCK, BLOCK), F32),
            V((rows, ret_cols), BF16),
            V((rows, ret_cols), BF16),
            V((rows, ret_cols), BF16),
            V((rows, ret_cols), BF16),
            V((HALO + rows, pool_cols), BF16),
            V((rows, ret_cols), F32),
            V((both, HEAD_DIM, HEAD_DIM), F32),
            V((heads, HEAD_DIM, HEAD_DIM), F32),
            V((heads, HEAD_DIM, HEAD_DIM), BF16),
            V((sp_n, heads, HEAD_DIM, HEAD_DIM), BF16),
            V((tot_rows, HEAD_DIM), F32),
            V((sp_n, tot_rows, HEAD_DIM), F32),
            V((HALO, pool_cols), BF16),
            V((heads, HEAD_DIM, HEAD_DIM), F32),
            V((rows, pool_cols), BF16),
            V((rows, ret_cols), BF16),
            V((rows_out, tp_n * (ret_cols + pool_cols)), BF16),
            V((rows_out, w_out.shape[1]), F32),
            dma((n_chunks,)),
            dma((6,)),
            dma((sp_n,)),
            dma((sp_n,)),
            dma((sp_n,)),
            dma((sp_n,)),
            dma((2,)),
            dma((2, n_chunks)),
            dma((2, tp_n, rows_out // CHUNK)),
        ],
        compiler_params=pltpu.CompilerParams(
            collective_id=0, has_side_effects=True, vmem_limit_bytes=62 * 1024 * 1024
        ),
    )(
        tokens, w_query, w_key, w_value, w_gate, w_pool, norm_gain.reshape(1, ret_cols), log_decay,
        w_out, *(jnp.asarray(t) for t in tables),
    )


def solution(mesh):
    sp_n, tp_n = mesh.shape["sp"], mesh.shape["tp"]

    def whole(tokens, *rest):
        tables = rotary_tables(tokens.shape[0] // BLOCK)
        body = functools.partial(local, sp_n, tp_n, tables)
        return jax.shard_map(
            body, mesh=mesh, in_specs=in_specs, out_specs=out_specs, check_vma=False
        )(tokens, *rest)

    in_specs = (
        P("sp", None),
        P(None, "tp"),
        P(None, "tp"),
        P(None, "tp"),
        P(None, "tp"),
        P(None, "tp"),
        P("tp"),
        P("tp", "sp"),
        P(),
    )
    out_specs = P(("sp", "tp"), None)
    return whole
```

profile of v0, /device:TPU:16, one launch (start us, length us, event | category | flops | bytes accessed | tf_op | source)
XLA Modules:
  0.0 57.6 jit_solution(13390229377935629443)
XLA Ops:
  0.0 54.4 %layer.1 = bf16[512,2048]{1,0:T(8,128)(2,1)} custom-call(bf16[2048,2048]{1,0:T(8,128)(2,1)} %tokens.1, bf16[2048,256]{1,0:T(8,128)(2,1)} %wq.1, bf16[2048,256]{1,0:T(8,128)(2,1)} %wk.1, bf16[2048,256]{1,0:T(8,128)(2,1)} %wv.1, bf16[2048,256]{1,0:T(8,128)(2,1)} %wg.1, bf16[2048,256]{1,0:T(8,128)(2,1)} %wp.1, f32[1,256]{1,0:T(1,128)} %bitcast.1, ...), custom_call_target="tpu_custom_call" | custom-call | tf_op jit(solution)/shard_map/layer/pallas_call | solution.py:435
  54.4 3.2 %copy.15 = bf16[512,2048]{1,0:T(8,128)(2,1)} copy(bf16[512,2048]{1,0:T(8,128)(2,1)} %layer.1) | data formatting | bytes 4194304
where the time goes:
time: 57.8 us; the launch traced here: 57.6 us
  Pallas kernels  54.4 us (94%)
  local copies, waits for them, and re-layouts  3.16 us (5%)
    pallas_call x1, Pallas kernels, local(): pl.pallas_call(functools.partial(kernel, sp_n, tp_n), name='layer', out_s...  54.4 us
    unnamed x1, local copies, waits for them, and re-layouts  3.16 us

commit v1 on v0

--- a/solution.py
+++ b/solution.py
@@ -44,7 +44,7 @@
     out,
     tok_v, wq_v, wk_v, wv_v, wg_v, wp_v, wout_v,
     ld_s, cum_s, bend_s, reach_s, col_s,
-    k_s, v_s, q_s, g_s, pool_s, inner_s, before_s, state_s,
+    k_s, v_s, q_s, g_s, kr_s, qr_s, pool_s, inner_s, before_s, state_s,
     st_send, st_recv, tot_send, tot_recv, rim_recv, inc_s,
     pooled_s, gated_s, gath, acc_s,
     tok_sem, w_sem, st_ssem, st_rsem, tot_ssem, tot_rsem, rim_sem, mix_ssem, mix_rsem,
@@ -78,16 +78,16 @@
     load_q = load(wq, wq_v, w_sem.at[3])
     load_g = load(wg, wg_v, w_sem.at[4])
     load_o = load(wout, wout_v, w_sem.at[5])
+    load_p.start()
+    tok_copy(n_chunks - 1).start()
     load_k.start()
-    tok_copy(0).start()
     load_v.start()
 
     def start_tok(c, carry):
         tok_copy(c).start()
         return carry
 
-    lax.fori_loop(1, n_chunks, start_tok, 0)
-    load_p.start()
+    lax.fori_loop(0, n_chunks - 1, start_tok, 0)
 
     def greet_sp(d, carry):
         pl.semaphore_signal(barrier, inc=1, device_id=((sp + d) % sp_n, tp), device_id_type=MESH)
@@ -119,8 +119,6 @@
     tot_send[...] = jnp.zeros_like(tot_send)
     tot_send[0:heads, :] = jnp.exp(run)
     state_s[...] = jnp.zeros_like(state_s)
-    load_k.wait()
-    load_v.wait()
 
     def angles(n):
         at = pl.ds(sp * n_blocks + n, 1)
@@ -137,20 +135,48 @@
     def block_rows(n):
         return pl.ds(pl.multiple_of(n * BLOCK, BLOCK), BLOCK)
 
-    def kv_chunk(c, carry):
-        tok_copy(c).wait()
-        x = tok_v[chunk_rows(c), :]
-        key = mm(x, wk_v[...]).astype(BF16).astype(F32)
-        value = mm(x, wv_v[...]).astype(BF16)
-        v_s[chunk_rows(c), :] = value
-        for b in range(per_chunk):
-            n = c * per_chunk + b
+    load_p.wait()
+    tok_copy(n_chunks - 1).wait()
+
+    def pool_chunk(c):
+        at = pl.ds(pl.multiple_of(HALO + c * CHUNK, HALO), CHUNK)
+        pool_s[at, :] = mm(tok_v[chunk_rows(c), :], wp_v[...]).astype(BF16)
+
+    pool_chunk(n_chunks - 1)
+    pl.semaphore_wait(barrier, sp_n - 1 + tp_n - 1)
+    rim = pltpu.make_async_remote_copy(
+        src_ref=pool_s.at[pl.ds(rows, HALO)], dst_ref=rim_recv, send_sem=rim_sem.at[0],
+        recv_sem=rim_sem.at[1], device_id=((sp + 1) % sp_n, tp), device_id_type=MESH,
+    )
+
+    @pl.when(sp < sp_n - 1)
+    def _():
+        rim.start()
+
+    load_k.wait()
+    load_v.wait()
+
+    step = 2 * CHUNK if rows % (2 * CHUNK) == 0 else CHUNK
+    n_steps = rows // step
+
+    def step_rows(c):
+        return pl.ds(pl.multiple_of(c * step, step), step)
+
+    def kv_dots(c):
+        x = tok_v[step_rows(c), :]
+        return mm(x, wk_v[...]).astype(BF16), mm(x, wv_v[...]).astype(BF16)
+
+    def kv_blocks(c):
+        key = k_s[step_rows(c), :].astype(F32)
+        value = v_s[step_rows(c), :]
+        for b in range(step // BLOCK):
+            n = c * (step // BLOCK) + b
             cosine, sine = angles(n)
             for h in range(heads):
                 cols = slice(h * HEAD_DIM, (h + 1) * HEAD_DIM)
                 part = slice(b * BLOCK, (b + 1) * BLOCK)
                 k_rot = (turned(key[part, cols], cosine, sine) * scale).astype(BF16)
-                k_s[block_rows(n), cols] = k_rot
+                kr_s[block_rows(n), cols] = k_rot
                 at = n * heads + h
                 col = jnp.broadcast_to(cum_s[pl.ds(at, 1), :], (BLOCK, BLOCK)).T
                 col_s[at] = col
@@ -163,16 +189,35 @@
                 state = state_s[h]
                 before_s[at] = state
                 state_s[h] = state * jnp.exp(end) + update
-        return carry
-
-    lax.fori_loop(0, n_chunks, kv_chunk, 0)
+
+    def kv_store(c, pair):
+        k_s[step_rows(c), :] = pair[0]
+        v_s[step_rows(c), :] = pair[1]
+
+    def kv_chunk(c, carry):
+        tok_wait(c)
+        pair = kv_dots(c)
+        kv_blocks(c - 1)
+        kv_store(c, pair)
+        return carry
+
+    def tok_wait(c):
+        for i in range(step // CHUNK):
+            at = c * (step // CHUNK) + i
+
+            @pl.when(at < n_chunks - 1)
+            def _():
+                tok_copy(at).wait()
+
+    tok_wait(0)
+    kv_store(0, kv_dots(0))
+    lax.fori_loop(1, n_steps, kv_chunk, 0)
+    kv_blocks(n_steps - 1)
     load_q.start()
     load_g.start()
     load_o.start()
     for h in range(heads):
         st_send[h] = state_s[h].astype(BF16)
-
-    pl.semaphore_wait(barrier, sp_n - 1 + tp_n - 1)
 
     def state_copies(d):
         target = ((sp + d) % sp_n, tp)
@@ -199,22 +244,6 @@
 
     lax.fori_loop(1, sp_n - sp, send_state, 0)
 
-    load_p.wait()
-
-    def pool_chunk(c):
-        at = pl.ds(pl.multiple_of(HALO + c * CHUNK, HALO), CHUNK)
-        pool_s[at, :] = mm(tok_v[chunk_rows(c), :], wp_v[...]).astype(BF16)
-
-    pool_chunk(n_chunks - 1)
-    rim = pltpu.make_async_remote_copy(
-        src_ref=pool_s.at[pl.ds(rows, HALO)], dst_ref=rim_recv, send_sem=rim_sem.at[0],
-        recv_sem=rim_sem.at[1], device_id=((sp + 1) % sp_n, tp), device_id_type=MESH,
-    )
-
-    @pl.when(sp < sp_n - 1)
-    def _():
-        rim.start()
-
     def pool_step(c, carry):
         pool_chunk(c)
         return carry
@@ -288,28 +317,51 @@
     load_q.wait()
     load_g.wait()
 
-    def q_chunk(c, carry):
-        x = tok_v[chunk_rows(c), :]
-        query = mm(x, wq_v[...]).astype(BF16).astype(F32)
-        g_s[chunk_rows(c), :] = mm(x, wg_v[...]).astype(BF16)
-        for b in range(per_chunk):
-            n = c * per_chunk + b
+    def dest_rows(c):
+        return pl.ds(pl.multiple_of(c * rows_out, rows_out), rows_out)
+
+    def q_dots(c):
+        x = tok_v[dest_rows(c), :]
+        return mm(x, wq_v[...]).astype(BF16), mm(x, wg_v[...]).astype(BF16)
+
+    def q_blocks(c):
+        query = q_s[dest_rows(c), :].astype(F32)
+        for b in range(rows_out // BLOCK):
+            n = c * (rows_out // BLOCK) + b
             cosine, sine = angles(n)
             for h in range(heads):
                 cols = slice(h * HEAD_DIM, (h + 1) * HEAD_DIM)
                 q_rot = turned(query[b * BLOCK : (b + 1) * BLOCK, cols], cosine, sine).astype(BF16)
-                q_s[block_rows(n), cols] = q_rot
+                qr_s[block_rows(n), cols] = q_rot
                 at = n * heads + h
                 fade = jnp.exp(jnp.minimum(col_s[at] - cum_s[pl.ds(at, 1), :], 0.0))
                 scores = lax.dot_general(
-                    q_rot, k_s[block_rows(n), cols], (((1,), (1,)), ((), ())),
+                    q_rot, kr_s[block_rows(n), cols], (((1,), (1,)), ((), ())),
                     preferred_element_type=F32,
                 )
                 mixing = (scores * jnp.where(causal, fade, 0.0)).astype(BF16)
                 inner_s[block_rows(n), cols] = mm(mixing, v_s[block_rows(n), cols])
-        return carry
-
-    lax.fori_loop(0, n_chunks, q_chunk, 0)
+
+    def q_store(c, pair):
+        q_s[dest_rows(c), :] = pair[0]
+        g_s[dest_rows(c), :] = pair[1]
+
+    def chunk_of(t):
+        return (tp // 2 + 1 + t // 2) % chips * 2 + (tp + t + 1) % 2
+
+    def q_chunk(t, carry):
+        pair = q_dots(chunk_of(t))
+        q_blocks(chunk_of(t - 1))
+        q_store(chunk_of(t), pair)
+        return carry
+
+    def q_range(first, last):
+        q_store(chunk_of(first), q_dots(chunk_of(first)))
+        lax.fori_loop(first + 1, last, q_chunk, 0)
+        q_blocks(chunk_of(last - 1))
+
+    away = n_chunks - 2 * pieces
+    q_range(0, tp_n - 2)
 
     inc_s[...] = jnp.zeros_like(inc_s)
 
@@ -334,7 +386,7 @@
                 cols = slice(h * HEAD_DIM, (h + 1) * HEAD_DIM)
                 at = n * heads + h
                 state = (before_s[at] + reach_s[pl.ds(at, 1), :] * inc_s[h]).astype(BF16)
-                cross = mm(q_s[block_rows(n), cols], state) * jnp.exp(col_s[at])
+                cross = mm(qr_s[block_rows(n), cols], state) * jnp.exp(col_s[at])
                 kept = inner_s[block_rows(n), cols] + cross
                 centered = kept - jnp.mean(kept, axis=-1, keepdims=True)
                 power = jnp.mean(centered * centered, axis=-1, keepdims=True)
@@ -345,7 +397,9 @@
         hand_over(0, t, jnp.concatenate(parts, axis=0))
         return carry
 
-    lax.fori_loop(0, n_chunks, ret_send, 0)
+    lax.fori_loop(0, away, ret_send, 0)
+    q_range(tp_n - 2, tp_n)
+    lax.fori_loop(away, n_chunks, ret_send, 0)
 
     load_o.wait()
 
@@ -369,18 +423,14 @@
     def tile_cols(j):
         return pl.ds(pl.multiple_of(j * tile, tile), tile)
 
-    def pool_out(piece, carry):
+    for piece in range(pieces):
         wait_piece(1, piece)
 
-        def one(j, carry):
-            acc_s[chunk_rows(piece), tile_cols(j)] = mm(
-                gath[chunk_rows(piece), ret_width:], wout_v[ret_width:, tile_cols(j)]
-            )
-            return carry
-
-        return lax.fori_loop(0, width_out // tile, one, carry)
-
-    lax.fori_loop(0, pieces, pool_out, 0)
+    def pool_out(j, carry):
+        acc_s[:, tile_cols(j)] = mm(gath[:, ret_width:], wout_v[ret_width:, tile_cols(j)])
+        return carry
+
+    lax.fori_loop(0, width_out // tile, pool_out, 0)
 
     def ret_out(piece, carry):
         wait_piece(0, piece)
@@ -455,6 +505,8 @@
             V((rows, ret_cols), BF16),
             V((rows, ret_cols), BF16),
             V((rows, ret_cols), BF16),
+            V((rows, ret_cols), BF16),
+            V((rows, ret_cols), BF16),
             V((HALO + rows, pool_cols), BF16),
             V((rows, ret_cols), F32),
             V((both, HEAD_DIM, HEAD_DIM), F32),

time: 57.8 us -> 48.6 us (0.84)
  the two profiles are of different devices: /device:TPU:16 before, /device:TPU:0 now
where the time goes in v1:
time: 48.6 us; the launch traced here: 48.5 us
  Pallas kernels  45.3 us (93%)
  local copies, waits for them, and re-layouts  3.16 us (7%)
    pallas_call x1, Pallas kernels, local(): pl.pallas_call(functools.partial(kernel, sp_n, tp_n), name='layer', out_s...  45.3 us
    unnamed x1, local copies, waits for them, and re-layouts  3.16 us

profile of v1, /device:TPU:0, one launch (start us, length us, event | category | flops | bytes accessed | tf_op | source)
XLA Modules:
  0.0 48.5 jit_solution(7136202446382872327)
XLA Ops:
  0.0 45.3 %layer.1 = bf16[512,2048]{1,0:T(8,128)(2,1)} custom-call(bf16[2048,2048]{1,0:T(8,128)(2,1)} %tokens.1, bf16[2048,256]{1,0:T(8,128)(2,1)} %wq.1, bf16[2048,256]{1,0:T(8,128)(2,1)} %wk.1, bf16[2048,256]{1,0:T(8,128)(2,1)} %wv.1, bf16[2048,256]{1,0:T(8,128)(2,1)} %wg.1, bf16[2048,256]{1,0:T(8,128)(2,1)} %wp.1, f32[1,256]{1,0:T(1,128)} %bitcast.1, ...), custom_call_target="tpu_custom_call" | custom-call | tf_op jit(solution)/shard_map/layer/pallas_call | solution.py:485
  45.3 3.2 %copy.15 = bf16[512,2048]{1,0:T(8,128)(2,1)} copy(bf16[512,2048]{1,0:T(8,128)(2,1)} %layer.1) | data formatting | bytes 4194304
